TPU v7x, 32 devices: a whole 2x2x4 slice. The times are simulated.
32 devices in a mesh: sp: 4 (over y, x), tp: 8 (over z, core).
Axes of the slice: x: 2, y: 2, z: 4, core: 2. Of those that a mesh axis runs over, the one named last changes fastest.
Arguments:
- stream: bfloat16 [2048, 1024], P('sp', 'tp'), may hold values from -6 to 6
- gain_first: bfloat16 [1024], P('tp'), may hold values from 0.099609375 to 1.8984375
- query_first: bfloat16 [1024, 1024], P('sp', 'tp'), may hold values from -0.1875 to 0.1875
- key_first: bfloat16 [1024, 1024], P('sp', 'tp'), may hold values from -0.1875 to 0.1875
- value_first: bfloat16 [1024, 1024], P('sp', 'tp'), may hold values from -0.1875 to 0.1875
- offset_first: float32 [8, 15, 31], P('tp'), may hold values from -4 to 254
- gain_second: bfloat16 [1024], P('tp'), may hold values from 0.099609375 to 1.8984375
- query_second: bfloat16 [1024, 1024], P('sp', 'tp'), may hold values from -0.1875 to 0.1875
- key_second: bfloat16 [1024, 1024], P('sp', 'tp'), may hold values from -0.1875 to 0.1875
- value_second: bfloat16 [1024, 1024], P('sp', 'tp'), may hold values from -0.1875 to 0.1875
- offset_second: float32 [8, 15, 31], P('tp'), may hold values from -4 to 254
Outputs:
- result: bfloat16 [2048, 1024], P('sp', 'tp')
All inputs are finite; a program needn't handle non-finite values.
Results may differ from a plain program's by a relative error of at most 0.008.
Values may be sent and summed in bfloat16 or wider, within the bound.
A program may use at most 64 MiB of HBM per device.

v0:
```python
import jax
import jax.numpy as jnp
import numpy as np
from jax import lax
from jax.sharding import PartitionSpec as P

GRID_W = 64
epsilon = 1e-06


def padded_2(block, sides, width):
    for axis, dim in sides:
        count = lax.axis_size(axis)
        forward = [(i, i + 1) for i in range(count - 1)]
        backward = [(target, source) for source, target in forward]
        low = lax.ppermute(
            lax.slice_in_dim(block, block.shape[dim] - width, None, axis=dim), axis, forward
        )
        high = lax.ppermute(lax.slice_in_dim(block, 0, width, axis=dim), axis, backward)
        block = jnp.concatenate([low, block, high], axis=dim)
    return block


def attend(query, keys, values, table, row_start, total_rows):
    rows_here, width, heads, head_size = query.shape
    blocks = width // 16
    query_cols = np.arange(width).reshape(blocks, 16)
    window_start = np.clip(query_cols - 8, 0, width - 16)
    key_cols = np.clip(np.arange(blocks) * 16 - 8, 0, width - 32)[:, None] + np.arange(32)
    column_ok = (key_cols[:, None, :] >= window_start[:, :, None]) & (
        key_cols[:, None, :] < window_start[:, :, None] + 16
    )
    column_offset = np.clip(key_cols[:, None, :] - query_cols[:, :, None] + 15, 0, 30)
    column_bias = table[:, :, column_offset]
    mask = jnp.asarray(column_ok)[None, :, :, None, :]
    factor = head_size ** (-0.5)

    def one_row(index):
        grid_row = row_start + index
        first = jnp.clip(grid_row - 4, 0, total_rows - 8)
        local = first - row_start + 4
        key_block = lax.dynamic_slice_in_dim(keys, local, 8, 0)[:, key_cols]
        value_block = lax.dynamic_slice_in_dim(values, local, 8, 0)[:, key_cols]
        query_row = lax.dynamic_index_in_dim(query, index, 0, keepdims=False).reshape(
            blocks, 16, heads, head_size
        )
        scores = (
            jnp.einsum(
                "jqhe,mjkhe->hjqmk", query_row, key_block, preferred_element_type=jnp.float32
            )
            * factor
        )
        row_offset = first + jnp.arange(8, dtype=jnp.int32) - grid_row + 7
        row_bias = jnp.transpose(jnp.take(column_bias, row_offset, axis=1), (0, 2, 3, 1, 4))
        scores = jnp.where(mask, scores + row_bias, -1e30)
        weight = jax.nn.softmax(scores.reshape(heads, blocks, 16, 256), axis=-1)
        rounded = weight.astype(jnp.bfloat16).reshape(heads, blocks, 16, 8, 32)
        output = jnp.einsum(
            "hjqmk,mjkhe->jqhe", rounded, value_block, preferred_element_type=jnp.float32
        )
        return output.reshape(width, heads * head_size)

    return jax.vmap(one_row)(jnp.arange(rows_here, dtype=jnp.int32))


def layer(stream, gain, w_query, w_key, w_value, table):
    tokens_dev, local_width = stream.shape
    widened = stream.astype(jnp.float32)
    full_rows, full_gain = (
        lax.all_gather(stream, "tp", axis=1, tiled=True),
        lax.all_gather(gain, "tp", axis=0, tiled=True),
    )
    full_wide = full_rows.astype(jnp.float32)
    mean_square = jnp.mean(full_wide * full_wide, axis=-1, keepdims=True)
    normed = (full_wide * lax.rsqrt(mean_square + epsilon) * full_gain.astype(jnp.float32)).astype(
        jnp.bfloat16
    )
    pieces = (
        lax.all_gather(w_query, "sp", axis=0, tiled=True),
        lax.all_gather(w_key, "sp", axis=0, tiled=True),
        lax.all_gather(w_value, "sp", axis=0, tiled=True),
    )
    query, key_part, value_part = tuple(
        (jnp.dot(normed, piece, preferred_element_type=jnp.float32) for piece in pieces)
    )
    heads_dev = table.shape[0]
    rows_dev = tokens_dev // GRID_W
    shape = (rows_dev, GRID_W, heads_dev, local_width // heads_dev)
    query = query.astype(jnp.bfloat16).reshape(shape)
    paired = jnp.stack(
        [
            key_part.astype(jnp.bfloat16).reshape(shape),
            value_part.astype(jnp.bfloat16).reshape(shape),
        ]
    )
    padded = padded_2(paired, (("sp", 1),), 4)
    row_start = lax.axis_index("sp") * rows_dev
    output = attend(query, padded[0], padded[1], table, row_start, rows_dev * lax.axis_size("sp"))
    return (widened + output.reshape(tokens_dev, local_width)).astype(jnp.bfloat16)


def body(
    stream,
    gain_first,
    query_first,
    key_first,
    value_first,
    offset_first,
    gain_second,
    query_second,
    key_second,
    value_second,
    offset_second,
):
    middle = layer(stream, gain_first, query_first, key_first, value_first, offset_first)
    return layer(middle, gain_second, query_second, key_second, value_second, offset_second)


def solution(mesh):
    placed = (
        P("sp", "tp"),
        P("tp"),
        P("sp", "tp"),
        P("sp", "tp"),
        P("sp", "tp"),
        P("tp", None, None),
        P("tp"),
        P("sp", "tp"),
        P("sp", "tp"),
        P("sp", "tp"),
        P("tp", None, None),
    )
    return jax.shard_map(body, mesh=mesh, in_specs=placed, out_specs=P("sp", "tp"), check_vma=False)
```

profile of v0, /device:TPU:0, one launch (start us, length us, event | category | flops | bytes accessed | tf_op | source)
XLA Modules:
  0.0 178.0 jit_solution(1198748897134902003)
XLA Ops:
  6.5 0.7 all-gather.5.cloned.1.call-update
  7.3 13.6 %all-gather = bf16[8,1,128]{2,1,0:T(2,128)(2,1)S(1)} all-gather(bf16[1,1,128]{2,1,0:T(2,128)(2,1)} %bitcast.156), channel_id=1, replica_groups=mesh['sp'=4,'tp'=8] {'tp'}, dimensions={0}, use_global_device_ids=true | all-gather | bytes 2304 | tf_op jit(solution)/shard_map/all_gather | solution.py:71
  21.1 0.8 copy.58
  21.9 0.7 broadcast_clamp_fusion
  22.6 5.5 %gather_fusion.5 = f32[2048,15]{1,0:T(8,128)S(1)} fusion(f32[15,31]{0,1:T(8,128)S(1)} %bitcast.126, s32[2048]{0:T(1024)S(1)} %broadcast_clamp_fusion), kind=kCustom, calls=%fused_computation.7 | custom fusion | bytes 253952 | tf_op jit(solution)/shard_map/gather | solution.py:34
  28.1 0.6 copy.59
  28.7 0.7 gather_fusion.12
  29.5 9.0 %all_gather.32 = bf16[1024,128]{1,0:T(8,128)(2,1)S(1)} all-gather(bf16[256,128]{1,0:T(8,128)(2,1)S(1)} %copy-done.4), channel_id=1, replica_groups=mesh['sp'=4,'tp'=8] {'sp'}, dimensions={0}, use_global_device_ids=true | all-gather | bytes 327680 | tf_op jit(solution)/shard_map/all_gather | solution.py:80
  38.5 9.0 %all_gather.33 = bf16[1024,128]{1,0:T(8,128)(2,1)S(1)} all-gather(bf16[256,128]{1,0:T(8,128)(2,1)S(1)} %copy-done.5), channel_id=1, replica_groups=mesh['sp'=4,'tp'=8] {'sp'}, dimensions={0}, use_global_device_ids=true | all-gather | bytes 327680 | tf_op jit(solution)/shard_map/all_gather | solution.py:81
  47.5 8.4 %all_gather.34 = bf16[1024,128]{1,0:T(8,128)(2,1)S(1)} all-gather(bf16[256,128]{1,0:T(8,128)(2,1)S(1)} %copy-done.6), channel_id=1, replica_groups=mesh['sp'=4,'tp'=8] {'sp'}, dimensions={0}, use_global_device_ids=true | all-gather | bytes 327680 | tf_op jit(solution)/shard_map/all_gather | solution.py:79
  56.5 0.7 compare_and_fusion
  57.1 1.6 fusion
  58.7 1.7 convolution_convert_fusion.5
  61.0 3.0 %collective-permute-start = (bf16[2,4,64,1,128]{4,2,1,3,0:T(8,128)(2,1)S(1)}, bf16[2,4,64,1,128]{4,2,1,3,0:T(8,128)(2,1)S(1)}, u32[]{:S(2)}, u32[]{:S(2)}) collective-permute-start(bf16[2,4,64,1,128]{4,2,1,3,0:T(8,128)(2,1)S(1)} %get-tuple-element.12), channel_id=1, source_target_pairs={{0,8},{8,16},{16,24},{1,9},{9,17},{17,25},{2,10},{10,18},{18,26},{... | collective-permute-start | bytes 393224 | tf_op jit(solution)/shard_map/ppermute | solution.py:16
  64.1 1.3 collective-permute-start.1
  66.6 4.4 %collective-permute-done.1 = bf16[2,4,64,1,128]{4,2,1,3,0:T(8,128)(2,1)S(1)} collective-permute-done((bf16[2,4,64,1,128]{4,2,1,3,0:T(8,128)(2,1)S(1)}, bf16[2,4,64,1,128]{4,2,1,3,0:T(8,128)(2,1)S(1)}, u32[]{:S(2)}, u32[]{:S(2)}) %collective-permute-start.1) | collective-permute-done | bytes 131104 | tf_op jit(solution)/shard_map/ppermute | solution.py:19
  71.1 1.7 gather_fusion.3
  72.7 1.9 %copy.56 = bf16[8,8,64,128]{3,1,2,0:T(8,128)(2,1)S(1)} copy(bf16[8,8,64,128]{3,2,1,0:T(8,128)(2,1)} %gather_fusion.3) | data formatting | bytes 2097152 | tf_op jit(solution)/shard_map/vmap()/gather | solution.py:42
  74.6 2.7 %gather_fusion.4 = bf16[128,8,8,128]{3,2,1,0:T(8,128)(2,1)} fusion(bf16[8,8,64,128]{3,1,2,0:T(8,128)(2,1)S(1)} %copy.56, s32[1024]{0:T(1024)} %pad_clamp_fusion.1), kind=kCustom, calls=%fused_computation.6 | custom fusion | bytes 4194816 | tf_op jit(solution)/shard_map/vmap()/gather | solution.py:42
  77.3 4.5 %fusion.39 = (f32[8,4,16]{2,1,0:T(4,128)S(1)}, f32[8,1,4,16,8,32]{5,3,4,2,0,1:T(8,128)S(1)}) fusion(f32[8,1,8,4,16,32]{5,4,3,2,0,1:T(8,128)S(1)} %bitcast.130, pred[8,8]{1,0:T(8,128)(4,1)} %compare_and_fusion, bf16[8,4,16,128,1]{3,2,4,1,0:T(8,128)(2,1)S(1)} %bitcast.139, bf16[4,32,8,8,128]{4,3,2,1,0:T(8,128)(2,1)} %bitcast.135, ...), kind=kOutput, calls=%fused_computation.87 | convolution fusion | flops 34209280 | bytes 3280960 | tf_op jit(solution)/shard_map/vmap(jqhe,mjkhe->hjqmk)/dot_general | solution.py:48
  82.9 1.4 copy.61
  84.2 1.7 gather_fusion
  85.9 1.9 %copy.52 = bf16[8,8,64,128]{3,1,2,0:T(8,128)(2,1)S(1)} copy(bf16[8,8,64,128]{3,2,1,0:T(8,128)(2,1)} %gather_fusion) | data formatting | bytes 2097152 | tf_op jit(solution)/shard_map/vmap()/gather | solution.py:43
  87.8 2.5 %gather_fusion.1 = bf16[128,8,8,128]{3,2,1,0:T(8,128)(2,1)} fusion(bf16[8,8,64,128]{3,1,2,0:T(8,128)(2,1)S(1)} %copy.52, s32[1024]{0:T(1024)S(1)} %copy-done.10), kind=kCustom, calls=%fused_computation.3 | custom fusion | bytes 4194816 | tf_op jit(solution)/shard_map/vmap()/gather | solution.py:43
  90.4 2.4 %fusion.14 = f32[8,4,128,16,1]{2,3,4,1,0:T(8,128)S(1)} fusion(bf16[8,4,16,8,32]{2,3,4,1,0:T(8,128)(2,1)S(1)} %copy.61, bf16[4,32,8,8,128]{4,3,2,1,0:T(8,128)(2,1)} %bitcast.133), kind=kOutput, calls=%fused_computation.34 | convolution fusion | flops 33554432 | bytes 2621440 | tf_op jit(solution)/shard_map/vmap(hjqmk,mjkhe->jqhe)/dot_general | solution.py:58
  92.8 0.7 fusion.29
  93.6 8.6 %all-gather.1 = bf16[8,1,128]{2,1,0:T(2,128)(2,1)S(1)} all-gather(bf16[1,1,128]{2,1,0:T(2,128)(2,1)S(1)} %bitcast.157), channel_id=1, replica_groups=mesh['sp'=4,'tp'=8] {'tp'}, dimensions={0}, use_global_device_ids=true | all-gather | bytes 2304 | tf_op jit(solution)/shard_map/all_gather | solution.py:71
  102.3 5.5 %gather_fusion.11 = f32[2048,15]{1,0:T(8,128)S(1)} fusion(f32[15,31]{0,1:T(8,128)S(1)} %bitcast.127, s32[2048]{0:T(1024)S(1)} %broadcast_clamp_fusion), kind=kCustom, calls=%fused_computation.13 | custom fusion | bytes 253952 | tf_op jit(solution)/shard_map/gather | solution.py:34
  107.7 0.6 copy.69
  108.4 0.7 gather_fusion.13
  109.2 9.8 %all_gather.38 = bf16[1024,128]{1,0:T(8,128)(2,1)S(1)} all-gather(bf16[256,128]{1,0:T(8,128)(2,1)S(1)} %copy-done.7), channel_id=1, replica_groups=mesh['sp'=4,'tp'=8] {'sp'}, dimensions={0}, use_global_device_ids=true | all-gather | bytes 327680 | tf_op jit(solution)/shard_map/all_gather | solution.py:81
  119.0 7.5 %all_gather.37 = bf16[1024,128]{1,0:T(8,128)(2,1)S(1)} all-gather(bf16[256,128]{1,0:T(8,128)(2,1)S(1)} %copy-done.8), channel_id=1, replica_groups=mesh['sp'=4,'tp'=8] {'sp'}, dimensions={0}, use_global_device_ids=true | all-gather | bytes 327680 | tf_op jit(solution)/shard_map/all_gather | solution.py:80
  126.5 9.5 %all_gather.39 = bf16[1024,128]{1,0:T(8,128)(2,1)S(1)} all-gather(bf16[256,128]{1,0:T(8,128)(2,1)S(1)} %copy-done.9), channel_id=1, replica_groups=mesh['sp'=4,'tp'=8] {'sp'}, dimensions={0}, use_global_device_ids=true | all-gather | bytes 327680 | tf_op jit(solution)/shard_map/all_gather | solution.py:79
  136.0 1.6 fusion.3
  137.6 1.7 convolution_convert_fusion.1
  139.9 1.9 %collective-permute-start.2 = (bf16[2,4,64,1,128]{4,2,1,3,0:T(8,128)(2,1)S(1)}, bf16[2,4,64,1,128]{4,2,1,3,0:T(8,128)(2,1)S(1)}, u32[]{:S(2)}, u32[]{:S(2)}) collective-permute-start(bf16[2,4,64,1,128]{4,2,1,3,0:T(8,128)(2,1)S(1)} %get-tuple-element.10), channel_id=1, source_target_pairs={{0,8},{8,16},{16,24},{1,9},{9,17},{17,25},{2,10},{10,18},{18,26},{... | collective-permute-start | bytes 393224 | tf_op jit(solution)/shard_map/ppermute | solution.py:16
  141.8 1.3 collective-permute-start.3
  144.3 4.4 %collective-permute-done.3 = bf16[2,4,64,1,128]{4,2,1,3,0:T(8,128)(2,1)S(1)} collective-permute-done((bf16[2,4,64,1,128]{4,2,1,3,0:T(8,128)(2,1)S(1)}, bf16[2,4,64,1,128]{4,2,1,3,0:T(8,128)(2,1)S(1)}, u32[]{:S(2)}, u32[]{:S(2)}) %collective-permute-start.3) | collective-permute-done | bytes 131104 | tf_op jit(solution)/shard_map/ppermute | solution.py:19
  148.8 1.7 gather_fusion.9
  150.5 1.9 %copy.66 = bf16[8,8,64,128]{3,1,2,0:T(8,128)(2,1)S(1)} copy(bf16[8,8,64,128]{3,2,1,0:T(8,128)(2,1)} %gather_fusion.9) | data formatting | bytes 2097152 | tf_op jit(solution)/shard_map/vmap()/gather | solution.py:42
  152.4 2.5 %gather_fusion.10 = bf16[128,8,8,128]{3,2,1,0:T(8,128)(2,1)} fusion(bf16[8,8,64,128]{3,1,2,0:T(8,128)(2,1)S(1)} %copy.66, s32[1024]{0:T(1024)S(1)} %copy-done.11), kind=kCustom, calls=%fused_computation.12 | custom fusion | bytes 4194816 | tf_op jit(solution)/shard_map/vmap()/gather | solution.py:42
  154.9 4.5 %fusion.40 = (f32[8,4,16]{2,1,0:T(4,128)S(1)}, f32[8,1,4,16,8,32]{5,3,4,2,0,1:T(8,128)S(1)}) fusion(f32[8,1,8,4,16,32]{5,4,3,2,0,1:T(8,128)S(1)} %bitcast.131, pred[8,8]{1,0:T(8,128)(4,1)S(1)} %copy-done.14, bf16[8,4,16,128,1]{3,2,4,1,0:T(8,128)(2,1)S(1)} %bitcast.138, bf16[4,32,8,8,128]{4,3,2,1,0:T(8,128)(2,1)} %bitcast.134, ...), kind=kOutput, calls=%fused_computation.88 | convolution fusion | flops 34209280 | bytes 3280960 | tf_op jit(solution)/shard_map/vmap(jqhe,mjkhe->hjqmk)/dot_general | solution.py:48
  160.5 1.4 copy.71
  161.9 1.7 gather_fusion.6
  163.5 1.9 %copy.62 = bf16[8,8,64,128]{3,1,2,0:T(8,128)(2,1)S(1)} copy(bf16[8,8,64,128]{3,2,1,0:T(8,128)(2,1)} %gather_fusion.6) | data formatting | bytes 2097152 | tf_op jit(solution)/shard_map/vmap()/gather | solution.py:43
  165.4 2.5 %gather_fusion.7 = bf16[128,8,8,128]{3,2,1,0:T(8,128)(2,1)} fusion(bf16[8,8,64,128]{3,1,2,0:T(8,128)(2,1)S(1)} %copy.62, s32[1024]{0:T(1024)S(1)} %copy-done.11), kind=kCustom, calls=%fused_computation.9 | custom fusion | bytes 4194816 | tf_op jit(solution)/shard_map/vmap()/gather | solution.py:43
  168.0 2.4 %fusion.9 = f32[8,4,128,16,1]{2,3,4,1,0:T(8,128)S(1)} fusion(bf16[8,4,16,8,32]{2,3,4,1,0:T(8,128)(2,1)S(1)} %copy.71, bf16[4,32,8,8,128]{4,3,2,1,0:T(8,128)(2,1)} %bitcast.132), kind=kOutput, calls=%fused_computation.28 | convolution fusion | flops 33554432 | bytes 2621440 | tf_op jit(solution)/shard_map/vmap(hjqmk,mjkhe->jqhe)/dot_general | solution.py:58
  170.4 0.7 fusion.28
  (71 shorter events, 6.9 us)
Async XLA Ops:
  6.5 50.6 %all-gather.5.cloned.1.call-start = ((), (), s32[]{:S(2)}) async-start(), calls=%async_computation | async-start | bytes 1179648 | tf_op jit(solution)/shard_map/all_gather | solution.py:70
  7.3 128.7 %all-gather.7.cloned.1.call-start = ((), (), s32[]{:S(2)}) async-start(), calls=%async_computation.1 | async-start | bytes 1179648 | tf_op jit(solution)/shard_map/all_gather | solution.py:70
  28.7 0.8 copy-start.12
  28.7 0.8 copy-start.4
  28.7 9.8 %copy-start.5 = (bf16[256,128]{1,0:T(8,128)(2,1)S(1)}, bf16[256,128]{1,0:T(8,128)(2,1)}, u32[]{:S(2)}) copy-start(bf16[256,128]{1,0:T(8,128)(2,1)} %param.29) | copy-start | bytes 196612
  28.7 18.8 %copy-start.6 = (bf16[256,128]{1,0:T(8,128)(2,1)S(1)}, bf16[256,128]{1,0:T(8,128)(2,1)}, u32[]{:S(2)}) copy-start(bf16[256,128]{1,0:T(8,128)(2,1)} %param.27) | copy-start | bytes 196612
  28.7 27.1 %copy-start.17 = (s32[128]{0:T(128)S(1)}, s32[128]{0:T(128)}, u32[]{:S(2)}) copy-start(s32[128]{0:T(128)} %constant.239) | copy-start | bytes 1540
  57.1 3.3 %copy-start.1 = (bf16[512,1024]{1,0:T(8,128)(2,1)S(1)}, bf16[512,1024]{1,0:T(8,128)(2,1)}, u32[]{:S(2)}) copy-start(bf16[512,1024]{1,0:T(8,128)(2,1)} %all-gather.5.cloned.1.call-done) | copy-start | bytes 3145732
  61.0 5.6 %collective-permute-start = (bf16[2,4,64,1,128]{4,2,1,3,0:T(8,128)(2,1)S(1)}, bf16[2,4,64,1,128]{4,2,1,3,0:T(8,128)(2,1)S(1)}, u32[]{:S(2)}, u32[]{:S(2)}) collective-permute-start(bf16[2,4,64,1,128]{4,2,1,3,0:T(8,128)(2,1)S(1)} %get-tuple-element.12), channel_id=1, source_target_pairs={{0,8},{8,16},{16,24},{1,9},{9,17},{17,25},{2,10},{10,18},{18,26},{... | collective-permute-start | bytes 393224 | tf_op jit(solution)/shard_map/ppermute | solution.py:16
  64.1 6.9 %collective-permute-start.1 = (bf16[2,4,64,1,128]{4,2,1,3,0:T(8,128)(2,1)S(1)}, bf16[2,4,64,1,128]{4,2,1,3,0:T(8,128)(2,1)S(1)}, u32[]{:S(2)}, u32[]{:S(2)}) collective-permute-start(bf16[2,4,64,1,128]{4,2,1,3,0:T(8,128)(2,1)S(1)} %get-tuple-element.13), channel_id=1, source_target_pairs={{8,0},{16,8},{24,16},{9,1},{17,9},{25,17},{10,2},{18,10},{26,18},{... | collective-permute-start | bytes 393224 | tf_op jit(solution)/shard_map/ppermute | solution.py:19
  84.2 3.6 %copy-start.10 = (s32[1024]{0:T(1024)S(1)}, s32[1024]{0:T(1024)}, u32[]{:S(2)}) copy-start(s32[1024]{0:T(1024)} %pad_clamp_fusion.1) | copy-start | bytes 12292
  90.4 2.4 %copy-start.3 = (bf16[512,128]{1,0:T(8,128)(2,1)S(1)}, bf16[512,128]{1,0:T(8,128)(2,1)}, u32[]{:S(2)}) copy-start(bf16[512,128]{1,0:T(8,128)(2,1)} %param.25) | copy-start | bytes 393220
  90.4 3.2 %copy-start.16 = (bf16[128]{0:T(256)(128)(2,1)S(1)}, bf16[128]{0:T(256)(128)(2,1)}, u32[]{:S(2)}) copy-start(bf16[128]{0:T(256)(128)(2,1)} %param.31) | copy-start | bytes 772
  90.4 11.8 %copy-start.15 = (f32[1,15,31]{2,0,1:T(1,128)S(1)}, f32[1,15,31]{2,0,1:T(1,128)}, u32[]{:S(2)}) copy-start(f32[1,15,31]{2,0,1:T(1,128)} %param.35) | copy-start | bytes 5584
  102.3 6.1 %copy-start.13 = (s32[1024]{0:T(1024)S(1)}, s32[1024]{0:T(1024)}, u32[]{:S(2)}) copy-start(s32[1024]{0:T(1024)} %copy-done.12) | copy-start | bytes 12292
  108.4 0.8 copy-start.7
  108.4 10.7 %copy-start.8 = (bf16[256,128]{1,0:T(8,128)(2,1)S(1)}, bf16[256,128]{1,0:T(8,128)(2,1)}, u32[]{:S(2)}) copy-start(bf16[256,128]{1,0:T(8,128)(2,1)} %param.33) | copy-start | bytes 196612
  108.4 18.1 %copy-start.9 = (bf16[256,128]{1,0:T(8,128)(2,1)S(1)}, bf16[256,128]{1,0:T(8,128)(2,1)}, u32[]{:S(2)}) copy-start(bf16[256,128]{1,0:T(8,128)(2,1)} %param.32) | copy-start | bytes 196612
  136.0 3.3 %copy-start.2 = (bf16[512,1024]{1,0:T(8,128)(2,1)S(1)}, bf16[512,1024]{1,0:T(8,128)(2,1)}, u32[]{:S(2)}) copy-start(bf16[512,1024]{1,0:T(8,128)(2,1)} %all-gather.7.cloned.1.call-done) | copy-start | bytes 3145732
  139.9 4.4 %collective-permute-start.2 = (bf16[2,4,64,1,128]{4,2,1,3,0:T(8,128)(2,1)S(1)}, bf16[2,4,64,1,128]{4,2,1,3,0:T(8,128)(2,1)S(1)}, u32[]{:S(2)}, u32[]{:S(2)}) collective-permute-start(bf16[2,4,64,1,128]{4,2,1,3,0:T(8,128)(2,1)S(1)} %get-tuple-element.10), channel_id=1, source_target_pairs={{0,8},{8,16},{16,24},{1,9},{9,17},{17,25},{2,10},{10,18},{18,26},{... | collective-permute-start | bytes 393224 | tf_op jit(solution)/shard_map/ppermute | solution.py:16
  141.8 6.9 %collective-permute-start.3 = (bf16[2,4,64,1,128]{4,2,1,3,0:T(8,128)(2,1)S(1)}, bf16[2,4,64,1,128]{4,2,1,3,0:T(8,128)(2,1)S(1)}, u32[]{:S(2)}, u32[]{:S(2)}) collective-permute-start(bf16[2,4,64,1,128]{4,2,1,3,0:T(8,128)(2,1)S(1)} %get-tuple-element.11), channel_id=1, source_target_pairs={{8,0},{16,8},{24,16},{9,1},{17,9},{25,17},{10,2},{18,10},{26,18},{... | collective-permute-start | bytes 393224 | tf_op jit(solution)/shard_map/ppermute | solution.py:19
  148.8 3.6 %copy-start.11 = (s32[1024]{0:T(1024)S(1)}, s32[1024]{0:T(1024)}, u32[]{:S(2)}) copy-start(s32[1024]{0:T(1024)} %pad_clamp_fusion.1) | copy-start | bytes 12292
  152.4 2.6 %copy-start.14 = (pred[8,8]{1,0:T(8,128)(4,1)S(1)}, pred[8,8]{1,0:T(8,128)(4,1)}, u32[]{:S(2)}) copy-start(pred[8,8]{1,0:T(8,128)(4,1)} %compare_and_fusion) | copy-start | bytes 196
  168.0 2.4 %copy-start = (bf16[512,128]{1,0:T(8,128)(2,1)S(1)}, bf16[512,128]{1,0:T(8,128)(2,1)}, u32[]{:S(2)}) copy-start(bf16[512,128]{1,0:T(8,128)(2,1)} %fusion.29) | copy-start | bytes 393220
Sparse Core Ops, SparseCore 0:
  8.9 26.6 all-gather.4
  93.7 21.9 all-gather.6
where the time goes:
time: 179 us; the launch traced here: 178 us
  blocking collectives  75.3 us (42%)
  local copies, waits for them, and re-layouts  43.4 us (24%)
  matrix products  19.4 us (11%)
  between operations  13.8 us (8%)
  waiting for transfers between devices  9.68 us (5%)
  other arithmetic  8.83 us (5%)
  starting transfers between devices  7.59 us (4%)
    all_gather x2, blocking collectives, layer(): lax.all_gather(gain, 'tp', axis=0, tiled=True)  22.2 us
    all_gather x2, blocking collectives, layer(): lax.all_gather(w_value, 'sp', axis=0, tiled=True)  18.8 us
    all_gather x2, blocking collectives, layer(): lax.all_gather(w_query, 'sp', axis=0, tiled=True)  17.9 us
    all_gather x2, blocking collectives, layer(): lax.all_gather(w_key, 'sp', axis=0, tiled=True)  16.5 us
    gather x6, local copies, waits for them, and re-layouts, one_row(): key_block = lax.dynamic_slice_in_dim(keys, local, 8, 0)[:, key_cols]  12.4 us
    gather x6, local copies, waits for them, and re-layouts, one_row(): value_block = lax.dynamic_slice_in_dim(values, local, 8, 0)[:, key_cols]  12.3 us
    gather x4, local copies, waits for them, and re-layouts, attend(): column_bias = table[:, :, column_offset]  12.1 us
    dot_general x2, matrix products, one_row(): jnp.einsum('jqhe,mjkhe->hjqmk', query_row, key_block, preferred_element_t...  9.08 us
  transfers between devices with their start and end apart: 6, of which 4 were waited for; matrix products, arithmetic and copies ran while one was open for 10% of the time, Pallas kernels for 0%

commit v1 on v0

--- a/solution.py
+++ b/solution.py
@@ -3,6 +3,7 @@
 import numpy as np
 from jax import lax
 from jax.sharding import PartitionSpec as P
+from jax.lax import axis_index, axis_size, ppermute
 
 GRID_W = 64
 epsilon = 1e-06
@@ -75,9 +76,40 @@
     normed = (full_wide * lax.rsqrt(mean_square + epsilon) * full_gain.astype(jnp.float32)).astype(
         jnp.bfloat16
     )
+
+    def fix_cube(s0, mesh_ax, ndim_at=0):
+        e_next = axis_size(mesh_ax)
+        z1 = axis_index(mesh_ax)
+        mixed_arr, x_next, k_now = (e_next, z1, s0.shape[ndim_at])
+        seen_now = range(mixed_arr)
+        clean = map(lambda idx: (idx, (idx + 1) % mixed_arr), seen_now)
+        chunks = list(clean)
+        carry_in = range(mixed_arr)
+        tmp = map(lambda idx: (idx, (idx - 1) % mixed_arr), carry_in)
+        by_rank = list(tmp)
+        d_next = jnp.zeros(
+            (*s0.shape[:ndim_at], mixed_arr * k_now, *s0.shape[ndim_at + 1 :]), s0.dtype
+        )
+        d_next = lax.dynamic_update_slice_in_dim(d_next, s0, x_next * k_now, axis=ndim_at)
+        current_value = piece_next = s0
+        v_next = mixed_arr // 2
+        h = 1
+        while h < v_next + 1:
+            current_value = ppermute(current_value, mesh_ax, chunks)
+            d_next = lax.dynamic_update_slice_in_dim(
+                d_next, current_value, (x_next - h) % mixed_arr * k_now, axis=ndim_at
+            )
+            if h < mixed_arr - v_next:
+                piece_next = ppermute(piece_next, mesh_ax, by_rank)
+                d_next = lax.dynamic_update_slice_in_dim(
+                    d_next, piece_next, (x_next + h) % mixed_arr * k_now, axis=ndim_at
+                )
+            h = h + 1
+        return d_next
+
     pieces = (
         lax.all_gather(w_query, "sp", axis=0, tiled=True),
-        lax.all_gather(w_key, "sp", axis=0, tiled=True),
+        fix_cube(w_key, "sp"),
         lax.all_gather(w_value, "sp", axis=0, tiled=True),
     )
     query, key_part, value_part = tuple(

time: 179 us -> 181 us (1.011)
  blocking collectives: 75.3 us -> 55.3 us
  starting transfers between devices: 7.59 us -> 18.3 us
  waiting for transfers between devices: 9.68 us -> 16.1 us
  local copies, waits for them, and re-layouts: 43.4 us -> 45.9 us
    all_gather x2 -> x0, blocking collectives: 16.5 us -> none  [layer(): lax.all_gather(w_key, 'sp', axis=0, tiled=True)]
    ppermute x0 -> x6, starting transfers between devices: none -> 10.5 us  [the longest x4 9.46 us: fix_cube(): current_value = ppermute(current_value, mesh_ax, chunks)]
    ppermute x0 -> x6, waiting for transfers between devices: none -> 6.21 us  [the longest x4 6.21 us: fix_cube(): current_value = ppermute(current_value, mesh_ax, chunks)]
    all_gather x2, blocking collectives: 17.9 us -> 15.8 us  [layer(): lax.all_gather(w_query, 'sp', axis=0, tiled=True)]
  transfers between devices with their start and end apart: 6 -> 12, of which waited for: 4 -> 6; matrix products, arithmetic and copies ran while one was open for 10% -> 12% of each run, Pallas kernels for 0% -> 0%
where the time goes in v1:
time: 181 us; the launch traced here: 179 us
  blocking collectives  55.3 us (31%)
  local copies, waits for them, and re-layouts  45.9 us (25%)
  matrix products  19.4 us (11%)
  starting transfers between devices  18.3 us (10%)
  waiting for transfers between devices  16.1 us (9%)
  between operations  13.8 us (8%)
  other arithmetic  10.4 us (6%)
    all_gather x2, blocking collectives, layer(): lax.all_gather(gain, 'tp', axis=0, tiled=True)  20.6 us
    all_gather x2, blocking collectives, layer(): lax.all_gather(w_value, 'sp', axis=0, tiled=True)  18.9 us
    all_gather x2, blocking collectives, layer(): lax.all_gather(w_query, 'sp', axis=0, tiled=True)  15.8 us
    gather x6, local copies, waits for them, and re-layouts, one_row(): key_block = lax.dynamic_slice_in_dim(keys, local, 8, 0)[:, key_cols]  12.4 us
    gather x6, local copies, waits for them, and re-layouts, one_row(): value_block = lax.dynamic_slice_in_dim(values, local, 8, 0)[:, key_cols]  12.2 us
    gather x4, local copies, waits for them, and re-layouts, attend(): column_bias = table[:, :, column_offset]  12.1 us
    ppermute x4, starting transfers between devices, fix_cube(): current_value = ppermute(current_value, mesh_ax, chunks)  9.46 us
    dot_general x2, matrix products, one_row(): jnp.einsum('jqhe,mjkhe->hjqmk', query_row, key_block, preferred_element_t...  9.08 us
  transfers between devices with their start and end apart: 12, of which 6 were waited for; matrix products, arithmetic and copies ran while one was open for 12% of the time, Pallas kernels for 0%

profile of v1, /device:TPU:0, one launch (start us, length us, event | category | flops | bytes accessed | tf_op | source)
XLA Modules:
  0.0 179.3 jit_solution(10947888615254876447)
XLA Ops:
  7.3 3.0 %collective-permute-start = (bf16[256,128]{1,0:T(8,128)(2,1)}, bf16[256,128]{1,0:T(8,128)(2,1)S(1)}, u32[]{:S(2)}, u32[]{:S(2)}) collective-permute-start(bf16[256,128]{1,0:T(8,128)(2,1)} %param.28), channel_id=1, source_target_pairs={{0,8},{8,16},{16,24},{24,0},{1,9},{9,17},{17,25},{25,1},{2,10},{10... | collective-permute-start | bytes 196616 | tf_op jit(solution)/shard_map/ppermute | solution.py:98
  10.3 1.0 collective-permute-start.1
  11.5 1.2 pad_clamp_fusion.1
  12.8 0.9 constant_dynamic-update-slice_fusion.7
  15.0 9.4 %all_gather.26 = bf16[1024,128]{1,0:T(8,128)(2,1)S(1)} all-gather(bf16[256,128]{1,0:T(8,128)(2,1)} %param.29), channel_id=1, replica_groups=mesh['sp'=4,'tp'=8] {'sp'}, dimensions={0}, use_global_device_ids=true | all-gather | bytes 327680 | tf_op jit(solution)/shard_map/all_gather | solution.py:113
  24.4 12.1 %all-gather = bf16[8,1,128]{2,1,0:T(2,128)(2,1)S(1)} all-gather(bf16[1,1,128]{2,1,0:T(2,128)(2,1)} %bitcast.156), channel_id=1, replica_groups=mesh['sp'=4,'tp'=8] {'tp'}, dimensions={0}, use_global_device_ids=true | all-gather | bytes 2304 | tf_op jit(solution)/shard_map/all_gather | solution.py:72
  36.6 0.8 copy.58
  37.4 5.5 %gather_fusion.5 = f32[2048,15]{1,0:T(8,128)S(1)} fusion(f32[15,31]{0,1:T(8,128)S(1)} %bitcast.127, s32[2048]{0:T(1024)S(1)} %broadcast_clamp_fusion), kind=kCustom, calls=%fused_computation.7 | custom fusion | bytes 253952 | tf_op jit(solution)/shard_map/gather | solution.py:35
  44.3 8.3 %all_gather.27 = bf16[1024,128]{1,0:T(8,128)(2,1)S(1)} all-gather(bf16[256,128]{1,0:T(8,128)(2,1)S(1)} %copy-done.5), channel_id=1, replica_groups=mesh['sp'=4,'tp'=8] {'sp'}, dimensions={0}, use_global_device_ids=true | all-gather | bytes 327680 | tf_op jit(solution)/shard_map/all_gather | solution.py:111
  52.6 1.2 collective-permute-start.2
  53.9 0.9 constant_dynamic-update-slice_fusion.5
  54.7 3.1 %collective-permute-done.2 = bf16[256,128]{1,0:T(8,128)(2,1)S(1)} collective-permute-done((bf16[256,128]{1,0:T(8,128)(2,1)S(1)}, bf16[256,128]{1,0:T(8,128)(2,1)S(1)}, u32[]{:S(2)}, u32[]{:S(2)}) %collective-permute-start.2) | collective-permute-done | bytes 65568 | tf_op jit(solution)/shard_map/ppermute | solution.py:98
  57.9 1.6 fusion
  59.5 1.7 convolution_convert_fusion.5
  61.8 2.2 %collective-permute-start.3 = (bf16[2,4,64,1,128]{4,2,1,3,0:T(8,128)(2,1)S(1)}, bf16[2,4,64,1,128]{4,2,1,3,0:T(8,128)(2,1)S(1)}, u32[]{:S(2)}, u32[]{:S(2)}) collective-permute-start(bf16[2,4,64,1,128]{4,2,1,3,0:T(8,128)(2,1)S(1)} %get-tuple-element.12), channel_id=1, source_target_pairs={{0,8},{8,16},{16,24},{1,9},{9,17},{17,25},{2,10},{10,18},{18,26},{... | collective-permute-start | bytes 393224 | tf_op jit(solution)/shard_map/ppermute | solution.py:17
  64.0 1.3 collective-permute-start.4
  67.1 4.2 %collective-permute-done.4 = bf16[2,4,64,1,128]{4,2,1,3,0:T(8,128)(2,1)} collective-permute-done((bf16[2,4,64,1,128]{4,2,1,3,0:T(8,128)(2,1)S(1)}, bf16[2,4,64,1,128]{4,2,1,3,0:T(8,128)(2,1)}, u32[]{:S(2)}, u32[]{:S(2)}) %collective-permute-start.4) | collective-permute-done | bytes 131104 | tf_op jit(solution)/shard_map/ppermute | solution.py:20
  71.3 1.0 pad_maximum_fusion
  72.4 1.7 gather_fusion.3
  74.0 1.9 %copy.56 = bf16[8,8,64,128]{3,1,2,0:T(8,128)(2,1)S(1)} copy(bf16[8,8,64,128]{3,2,1,0:T(8,128)(2,1)} %gather_fusion.3) | data formatting | bytes 2097152 | tf_op jit(solution)/shard_map/vmap()/gather | solution.py:43
  76.0 2.7 %gather_fusion.4 = bf16[128,8,8,128]{3,2,1,0:T(8,128)(2,1)} fusion(bf16[8,8,64,128]{3,1,2,0:T(8,128)(2,1)S(1)} %copy.56, s32[1024]{0:T(1024)} %pad_clamp_fusion.1), kind=kCustom, calls=%fused_computation.6 | custom fusion | bytes 4194816 | tf_op jit(solution)/shard_map/vmap()/gather | solution.py:43
  78.6 4.5 %fusion.39 = (f32[8,4,16]{2,1,0:T(4,128)S(1)}, f32[8,1,4,16,8,32]{5,3,4,2,0,1:T(8,128)S(1)}) fusion(f32[8,1,8,4,16,32]{5,4,3,2,0,1:T(8,128)S(1)} %bitcast.131, pred[8,8]{1,0:T(8,128)(4,1)} %compare_and_fusion, bf16[8,4,16,128,1]{3,2,4,1,0:T(8,128)(2,1)S(1)} %bitcast.139, bf16[4,32,8,8,128]{4,3,2,1,0:T(8,128)(2,1)} %bitcast.135, ...), kind=kOutput, calls=%fused_computation.95 | convolution fusion | flops 34209280 | bytes 3280960 | tf_op jit(solution)/shard_map/vmap(jqhe,mjkhe->hjqmk)/dot_general | solution.py:49
  84.2 1.4 copy.61
  85.5 1.7 gather_fusion
  87.2 1.9 %copy.52 = bf16[8,8,64,128]{3,1,2,0:T(8,128)(2,1)S(1)} copy(bf16[8,8,64,128]{3,2,1,0:T(8,128)(2,1)} %gather_fusion) | data formatting | bytes 2097152 | tf_op jit(solution)/shard_map/vmap()/gather | solution.py:44
  89.1 2.5 %gather_fusion.1 = bf16[128,8,8,128]{3,2,1,0:T(8,128)(2,1)} fusion(bf16[8,8,64,128]{3,1,2,0:T(8,128)(2,1)S(1)} %copy.52, s32[1024]{0:T(1024)S(1)} %copy-done.9), kind=kCustom, calls=%fused_computation.3 | custom fusion | bytes 4194816 | tf_op jit(solution)/shard_map/vmap()/gather | solution.py:44
  91.7 2.4 %fusion.14 = f32[8,4,128,16,1]{2,3,4,1,0:T(8,128)S(1)} fusion(bf16[8,4,16,8,32]{2,3,4,1,0:T(8,128)(2,1)S(1)} %copy.61, bf16[4,32,8,8,128]{4,3,2,1,0:T(8,128)(2,1)} %bitcast.133), kind=kOutput, calls=%fused_computation.34 | convolution fusion | flops 33554432 | bytes 2621440 | tf_op jit(solution)/shard_map/vmap(hjqmk,mjkhe->jqhe)/dot_general | solution.py:59
  94.9 3.1 %collective-permute-start.5 = (bf16[256,128]{1,0:T(8,128)(2,1)S(1)}, bf16[256,128]{1,0:T(8,128)(2,1)S(1)}, u32[]{:S(2)}, u32[]{:S(2)}) collective-permute-start(bf16[256,128]{1,0:T(8,128)(2,1)S(1)} %copy-done.8), channel_id=1, source_target_pairs={{0,8},{8,16},{16,24},{24,0},{1,9},{9,17},{17,25},{25,1},{2,10},{10... | collective-permute-start | bytes 196616 | tf_op jit(solution)/shard_map/ppermute | solution.py:98
  98.1 9.5 %all_gather.30 = bf16[1024,128]{1,0:T(8,128)(2,1)S(1)} all-gather(bf16[256,128]{1,0:T(8,128)(2,1)S(1)} %copy-done.6), channel_id=1, replica_groups=mesh['sp'=4,'tp'=8] {'sp'}, dimensions={0}, use_global_device_ids=true | all-gather | bytes 327680 | tf_op jit(solution)/shard_map/all_gather | solution.py:113
  107.6 8.4 %all-gather.1 = bf16[8,1,128]{2,1,0:T(2,128)(2,1)S(1)} all-gather(bf16[1,1,128]{2,1,0:T(2,128)(2,1)S(1)} %bitcast.157), channel_id=1, replica_groups=mesh['sp'=4,'tp'=8] {'tp'}, dimensions={0}, use_global_device_ids=true | all-gather | bytes 2304 | tf_op jit(solution)/shard_map/all_gather | solution.py:72
  116.1 5.5 %gather_fusion.11 = f32[2048,15]{1,0:T(8,128)S(1)} fusion(f32[15,31]{0,1:T(8,128)S(1)} %bitcast.126, s32[2048]{0:T(1024)S(1)} %broadcast_clamp_fusion), kind=kCustom, calls=%fused_computation.13 | custom fusion | bytes 253952 | tf_op jit(solution)/shard_map/gather | solution.py:35
  123.1 7.5 %all_gather.31 = bf16[1024,128]{1,0:T(8,128)(2,1)S(1)} all-gather(bf16[256,128]{1,0:T(8,128)(2,1)S(1)} %copy-done.7), channel_id=1, replica_groups=mesh['sp'=4,'tp'=8] {'sp'}, dimensions={0}, use_global_device_ids=true | all-gather | bytes 327680 | tf_op jit(solution)/shard_map/all_gather | solution.py:111
  130.6 2.1 %collective-permute-start.7 = (bf16[256,128]{1,0:T(8,128)(2,1)S(1)}, bf16[256,128]{1,0:T(8,128)(2,1)S(1)}, u32[]{:S(2)}, u32[]{:S(2)}) collective-permute-start(bf16[256,128]{1,0:T(8,128)(2,1)S(1)} %collective-permute-done.5), channel_id=1, source_target_pairs={{0,8},{8,16},{16,24},{24,0},{1,9},{9,17},{17,25},{25,1},{2,10},{10... | collective-permute-start | bytes 196616 | tf_op jit(solution)/shard_map/ppermute | solution.py:98
  132.7 3.1 %collective-permute-done.7 = bf16[256,128]{1,0:T(8,128)(2,1)S(1)} collective-permute-done((bf16[256,128]{1,0:T(8,128)(2,1)S(1)}, bf16[256,128]{1,0:T(8,128)(2,1)S(1)}, u32[]{:S(2)}, u32[]{:S(2)}) %collective-permute-start.7) | collective-permute-done | bytes 65568 | tf_op jit(solution)/shard_map/ppermute | solution.py:98
  135.9 1.6 fusion.3
  137.5 1.7 convolution_convert_fusion.1
  139.8 3.0 %collective-permute-start.8 = (bf16[2,4,64,1,128]{4,2,1,3,0:T(8,128)(2,1)S(1)}, bf16[2,4,64,1,128]{4,2,1,3,0:T(8,128)(2,1)S(1)}, u32[]{:S(2)}, u32[]{:S(2)}) collective-permute-start(bf16[2,4,64,1,128]{4,2,1,3,0:T(8,128)(2,1)S(1)} %get-tuple-element.10), channel_id=1, source_target_pairs={{0,8},{8,16},{16,24},{1,9},{9,17},{17,25},{2,10},{10,18},{18,26},{... | collective-permute-start | bytes 393224 | tf_op jit(solution)/shard_map/ppermute | solution.py:17
  142.8 1.3 collective-permute-start.9
  145.3 4.7 %collective-permute-done.9 = bf16[2,4,64,1,128]{4,2,1,3,0:T(8,128)(2,1)S(1)} collective-permute-done((bf16[2,4,64,1,128]{4,2,1,3,0:T(8,128)(2,1)S(1)}, bf16[2,4,64,1,128]{4,2,1,3,0:T(8,128)(2,1)S(1)}, u32[]{:S(2)}, u32[]{:S(2)}) %collective-permute-start.9) | collective-permute-done | bytes 131104 | tf_op jit(solution)/shard_map/ppermute | solution.py:20
  150.1 1.7 gather_fusion.9
  151.8 1.9 %copy.66 = bf16[8,8,64,128]{3,1,2,0:T(8,128)(2,1)S(1)} copy(bf16[8,8,64,128]{3,2,1,0:T(8,128)(2,1)} %gather_fusion.9) | data formatting | bytes 2097152 | tf_op jit(solution)/shard_map/vmap()/gather | solution.py:43
  153.7 2.5 %gather_fusion.10 = bf16[128,8,8,128]{3,2,1,0:T(8,128)(2,1)} fusion(bf16[8,8,64,128]{3,1,2,0:T(8,128)(2,1)S(1)} %copy.66, s32[1024]{0:T(1024)S(1)} %copy-done.10), kind=kCustom, calls=%fused_computation.12 | custom fusion | bytes 4194816 | tf_op jit(solution)/shard_map/vmap()/gather | solution.py:43
  156.3 4.5 %fusion.40 = (f32[8,4,16]{2,1,0:T(4,128)S(1)}, f32[8,1,4,16,8,32]{5,3,4,2,0,1:T(8,128)S(1)}) fusion(f32[8,1,8,4,16,32]{5,4,3,2,0,1:T(8,128)S(1)} %bitcast.130, pred[8,8]{1,0:T(8,128)(4,1)S(1)} %copy-done.13, bf16[8,4,16,128,1]{3,2,4,1,0:T(8,128)(2,1)S(1)} %bitcast.138, bf16[4,32,8,8,128]{4,3,2,1,0:T(8,128)(2,1)} %bitcast.134, ...), kind=kOutput, calls=%fused_computation.96 | convolution fusion | flops 34209280 | bytes 3280960 | tf_op jit(solution)/shard_map/vmap(jqhe,mjkhe->hjqmk)/dot_general | solution.py:49
  161.8 1.4 copy.71
  163.2 1.7 gather_fusion.6
  164.9 1.9 %copy.62 = bf16[8,8,64,128]{3,1,2,0:T(8,128)(2,1)S(1)} copy(bf16[8,8,64,128]{3,2,1,0:T(8,128)(2,1)} %gather_fusion.6) | data formatting | bytes 2097152 | tf_op jit(solution)/shard_map/vmap()/gather | solution.py:44
  166.8 2.5 %gather_fusion.7 = bf16[128,8,8,128]{3,2,1,0:T(8,128)(2,1)} fusion(bf16[8,8,64,128]{3,1,2,0:T(8,128)(2,1)S(1)} %copy.62, s32[1024]{0:T(1024)S(1)} %copy-done.10), kind=kCustom, calls=%fused_computation.9 | custom fusion | bytes 4194816 | tf_op jit(solution)/shard_map/vmap()/gather | solution.py:44
  169.3 2.4 %fusion.9 = f32[8,4,128,16,1]{2,3,4,1,0:T(8,128)S(1)} fusion(bf16[8,4,16,8,32]{2,3,4,1,0:T(8,128)(2,1)S(1)} %copy.71, bf16[4,32,8,8,128]{4,3,2,1,0:T(8,128)(2,1)} %bitcast.132), kind=kOutput, calls=%fused_computation.28 | convolution fusion | flops 33554432 | bytes 2621440 | tf_op jit(solution)/shard_map/vmap(hjqmk,mjkhe->jqhe)/dot_general | solution.py:59
  (87 shorter events, 13.2 us)
Async XLA Ops:
  6.5 51.3 %all-gather.5.cloned.1.call-start = ((), (), s32[]{:S(2)}) async-start(), calls=%async_computation | async-start | bytes 1179648 | tf_op jit(solution)/shard_map/all_gather | solution.py:71
  7.3 128.6 %all-gather.7.cloned.1.call-start = ((), (), s32[]{:S(2)}) async-start(), calls=%async_computation.1 | async-start | bytes 1179648 | tf_op jit(solution)/shard_map/all_gather | solution.py:71
  7.3 45.3 %collective-permute-start = (bf16[256,128]{1,0:T(8,128)(2,1)}, bf16[256,128]{1,0:T(8,128)(2,1)S(1)}, u32[]{:S(2)}, u32[]{:S(2)}) collective-permute-start(bf16[256,128]{1,0:T(8,128)(2,1)} %param.28), channel_id=1, source_target_pairs={{0,8},{8,16},{16,24},{24,0},{1,9},{9,17},{17,25},{25,1},{2,10},{10... | collective-permute-start | bytes 196616 | tf_op jit(solution)/shard_map/ppermute | solution.py:98
  10.3 43.6 %collective-permute-start.1 = (bf16[256,128]{1,0:T(8,128)(2,1)}, bf16[256,128]{1,0:T(8,128)(2,1)}, u32[]{:S(2)}, u32[]{:S(2)}) collective-permute-start(bf16[256,128]{1,0:T(8,128)(2,1)} %param.28), channel_id=1, source_target_pairs={{0,24},{8,0},{16,8},{24,16},{1,25},{9,1},{17,9},{25,17},{2,26},{10... | collective-permute-start | bytes 196616 | tf_op jit(solution)/shard_map/ppermute | solution.py:103
  12.8 30.7 %copy-start.11 = (s32[1024]{0:T(1024)}, s32[1024]{0:T(1024)S(1)}, u32[]{:S(2)}) copy-start(s32[1024]{0:T(1024)S(1)} %pad_clamp_fusion) | copy-start | bytes 12292
  43.5 0.8 copy-start.5
  52.6 5.2 %collective-permute-start.2 = (bf16[256,128]{1,0:T(8,128)(2,1)S(1)}, bf16[256,128]{1,0:T(8,128)(2,1)S(1)}, u32[]{:S(2)}, u32[]{:S(2)}) collective-permute-start(bf16[256,128]{1,0:T(8,128)(2,1)S(1)} %collective-permute-done), channel_id=1, source_target_pairs={{0,8},{8,16},{16,24},{24,0},{1,9},{9,17},{17,25},{25,1},{2,10},{10... | collective-permute-start | bytes 196616 | tf_op jit(solution)/shard_map/ppermute | solution.py:98
  57.9 3.3 %copy-start.1 = (bf16[512,1024]{1,0:T(8,128)(2,1)S(1)}, bf16[512,1024]{1,0:T(8,128)(2,1)}, u32[]{:S(2)}) copy-start(bf16[512,1024]{1,0:T(8,128)(2,1)} %all-gather.5.cloned.1.call-done) | copy-start | bytes 3145732
  61.8 4.7 %collective-permute-start.3 = (bf16[2,4,64,1,128]{4,2,1,3,0:T(8,128)(2,1)S(1)}, bf16[2,4,64,1,128]{4,2,1,3,0:T(8,128)(2,1)S(1)}, u32[]{:S(2)}, u32[]{:S(2)}) collective-permute-start(bf16[2,4,64,1,128]{4,2,1,3,0:T(8,128)(2,1)S(1)} %get-tuple-element.12), channel_id=1, source_target_pairs={{0,8},{8,16},{16,24},{1,9},{9,17},{17,25},{2,10},{10,18},{18,26},{... | collective-permute-start | bytes 393224 | tf_op jit(solution)/shard_map/ppermute | solution.py:17
  64.0 7.3 %collective-permute-start.4 = (bf16[2,4,64,1,128]{4,2,1,3,0:T(8,128)(2,1)S(1)}, bf16[2,4,64,1,128]{4,2,1,3,0:T(8,128)(2,1)}, u32[]{:S(2)}, u32[]{:S(2)}) collective-permute-start(bf16[2,4,64,1,128]{4,2,1,3,0:T(8,128)(2,1)S(1)} %get-tuple-element.13), channel_id=1, source_target_pairs={{8,0},{16,8},{24,16},{9,1},{17,9},{25,17},{10,2},{18,10},{26,18},{... | collective-permute-start | bytes 393224 | tf_op jit(solution)/shard_map/ppermute | solution.py:20
  66.5 0.7 copy-start.4
  85.5 3.6 %copy-start.9 = (s32[1024]{0:T(1024)S(1)}, s32[1024]{0:T(1024)}, u32[]{:S(2)}) copy-start(s32[1024]{0:T(1024)} %pad_clamp_fusion.1) | copy-start | bytes 12292
  91.7 2.5 %copy-start.3 = (bf16[512,128]{1,0:T(8,128)(2,1)S(1)}, bf16[512,128]{1,0:T(8,128)(2,1)}, u32[]{:S(2)}) copy-start(bf16[512,128]{1,0:T(8,128)(2,1)} %param.25) | copy-start | bytes 393220
  91.7 3.2 %copy-start.8 = (bf16[256,128]{1,0:T(8,128)(2,1)S(1)}, bf16[256,128]{1,0:T(8,128)(2,1)}, u32[]{:S(2)}) copy-start(bf16[256,128]{1,0:T(8,128)(2,1)} %param.33) | copy-start | bytes 196612
  91.7 6.4 %copy-start.6 = (bf16[256,128]{1,0:T(8,128)(2,1)S(1)}, bf16[256,128]{1,0:T(8,128)(2,1)}, u32[]{:S(2)}) copy-start(bf16[256,128]{1,0:T(8,128)(2,1)} %param.34) | copy-start | bytes 196612
  91.7 15.9 %copy-start.15 = (bf16[128]{0:T(256)(128)(2,1)S(1)}, bf16[128]{0:T(256)(128)(2,1)}, u32[]{:S(2)}) copy-start(bf16[128]{0:T(256)(128)(2,1)} %param.31) | copy-start | bytes 772
  91.7 24.4 %copy-start.14 = (f32[1,15,31]{2,0,1:T(1,128)S(1)}, f32[1,15,31]{2,0,1:T(1,128)}, u32[]{:S(2)}) copy-start(f32[1,15,31]{2,0,1:T(1,128)} %param.35) | copy-start | bytes 5584
  94.9 35.7 %collective-permute-start.5 = (bf16[256,128]{1,0:T(8,128)(2,1)S(1)}, bf16[256,128]{1,0:T(8,128)(2,1)S(1)}, u32[]{:S(2)}, u32[]{:S(2)}) collective-permute-start(bf16[256,128]{1,0:T(8,128)(2,1)S(1)} %copy-done.8), channel_id=1, source_target_pairs={{0,8},{8,16},{16,24},{24,0},{1,9},{9,17},{17,25},{25,1},{2,10},{10... | collective-permute-start | bytes 196616 | tf_op jit(solution)/shard_map/ppermute | solution.py:98
  98.0 34.7 %collective-permute-start.6 = (bf16[256,128]{1,0:T(8,128)(2,1)S(1)}, bf16[256,128]{1,0:T(8,128)(2,1)S(1)}, u32[]{:S(2)}, u32[]{:S(2)}) collective-permute-start(bf16[256,128]{1,0:T(8,128)(2,1)S(1)} %copy-done.8), channel_id=1, source_target_pairs={{0,24},{8,0},{16,8},{24,16},{1,25},{9,1},{17,9},{25,17},{2,26},{10... | collective-permute-start | bytes 196616 | tf_op jit(solution)/shard_map/ppermute | solution.py:103
  116.1 6.1 %copy-start.12 = (s32[1024]{0:T(1024)S(1)}, s32[1024]{0:T(1024)}, u32[]{:S(2)}) copy-start(s32[1024]{0:T(1024)} %copy-done.11) | copy-start | bytes 12292
  122.2 0.8 copy-start.7
  130.6 5.2 %collective-permute-start.7 = (bf16[256,128]{1,0:T(8,128)(2,1)S(1)}, bf16[256,128]{1,0:T(8,128)(2,1)S(1)}, u32[]{:S(2)}, u32[]{:S(2)}) collective-permute-start(bf16[256,128]{1,0:T(8,128)(2,1)S(1)} %collective-permute-done.5), channel_id=1, source_target_pairs={{0,8},{8,16},{16,24},{24,0},{1,9},{9,17},{17,25},{25,1},{2,10},{10... | collective-permute-start | bytes 196616 | tf_op jit(solution)/shard_map/ppermute | solution.py:98
  135.9 3.3 %copy-start.2 = (bf16[512,1024]{1,0:T(8,128)(2,1)S(1)}, bf16[512,1024]{1,0:T(8,128)(2,1)}, u32[]{:S(2)}) copy-start(bf16[512,1024]{1,0:T(8,128)(2,1)} %all-gather.7.cloned.1.call-done) | copy-start | bytes 3145732
  139.8 5.5 %collective-permute-start.8 = (bf16[2,4,64,1,128]{4,2,1,3,0:T(8,128)(2,1)S(1)}, bf16[2,4,64,1,128]{4,2,1,3,0:T(8,128)(2,1)S(1)}, u32[]{:S(2)}, u32[]{:S(2)}) collective-permute-start(bf16[2,4,64,1,128]{4,2,1,3,0:T(8,128)(2,1)S(1)} %get-tuple-element.10), channel_id=1, source_target_pairs={{0,8},{8,16},{16,24},{1,9},{9,17},{17,25},{2,10},{10,18},{18,26},{... | collective-permute-start | bytes 393224 | tf_op jit(solution)/shard_map/ppermute | solution.py:17
  142.8 7.2 %collective-permute-start.9 = (bf16[2,4,64,1,128]{4,2,1,3,0:T(8,128)(2,1)S(1)}, bf16[2,4,64,1,128]{4,2,1,3,0:T(8,128)(2,1)S(1)}, u32[]{:S(2)}, u32[]{:S(2)}) collective-permute-start(bf16[2,4,64,1,128]{4,2,1,3,0:T(8,128)(2,1)S(1)} %get-tuple-element.11), channel_id=1, source_target_pairs={{8,0},{16,8},{24,16},{9,1},{17,9},{25,17},{10,2},{18,10},{26,18},{... | collective-permute-start | bytes 393224 | tf_op jit(solution)/shard_map/ppermute | solution.py:20
  150.1 3.6 %copy-start.10 = (s32[1024]{0:T(1024)S(1)}, s32[1024]{0:T(1024)}, u32[]{:S(2)}) copy-start(s32[1024]{0:T(1024)} %pad_clamp_fusion.1) | copy-start | bytes 12292
  153.7 2.5 %copy-start.13 = (pred[8,8]{1,0:T(8,128)(4,1)S(1)}, pred[8,8]{1,0:T(8,128)(4,1)}, u32[]{:S(2)}) copy-start(pred[8,8]{1,0:T(8,128)(4,1)} %compare_and_fusion) | copy-start | bytes 196
  169.3 2.4 %copy-start = (bf16[512,128]{1,0:T(8,128)(2,1)S(1)}, bf16[512,128]{1,0:T(8,128)(2,1)}, u32[]{:S(2)}) copy-start(bf16[512,128]{1,0:T(8,128)(2,1)} %fusion.29) | copy-start | bytes 393220
Sparse Core Ops, SparseCore 0:
  8.9 26.8 all-gather.4
  95.0 22.5 all-gather.6
